TPU v7x, 32 devices: a whole 2x2x4 slice. The times are simulated.
32 devices in a mesh: fs: 4 (over y, x), tp: 8 (over z, core).
Axes of the slice: x: 2, y: 2, z: 4, core: 2. Of those that a mesh axis runs over, the one named last changes fastest.
Arguments:
- stream_in: bfloat16 [4096, 4096], P(('fs', 'tp')), may hold values from -6 to 6
- mixer_out: bfloat16 [4096, 4096], P(('fs', 'tp')), may hold values from -6 to 6
- mix_gain: float32 [4096], replicated, may hold values from 0.1 to 1.9
- pre_gain: float32 [4096], replicated, may hold values from 0.1 to 1.9
- gate_weight: float32 [4096, 6144], P('fs', 'tp'), may hold values from -0.09375 to 0.09375
- up_weight: float32 [4096, 6144], P('fs', 'tp'), may hold values from -0.09375 to 0.09375
- gate_scale: float32 [6144], P('tp'), may hold values from 0.5 to 2
- up_scale: float32 [6144], P('tp'), may hold values from 0.5 to 2
Outputs:
- hidden: bfloat16 [4096, 6144], P('fs', 'tp')
- stream: bfloat16 [4096, 4096], P(('fs', 'tp'))
All inputs are finite; a program needn't handle non-finite values.
Results may differ from a plain program's by a relative error of at most 0.0082.
Values may be sent and summed in bfloat16 or wider, within the bound.
A program may use at most 128 MiB of HBM per device.

v0:
```python
import jax
import jax.numpy as jnp
from jax import lax
from jax.sharding import PartitionSpec as P

epsilon = 1e-06


def rms_scaled(values, gain):
    return values * lax.rsqrt(jnp.mean(values * values, axis=-1, keepdims=True) + epsilon) * gain


def on_device(
    stream_in, mixer_out, mix_gain, pre_gain, gate_weight, up_weight, gate_scale, up_scale
):
    mixed = stream_in.astype(jnp.float32) + rms_scaled(mixer_out.astype(jnp.float32), mix_gain)
    stream = mixed.astype(jnp.bfloat16)
    normed = rms_scaled(stream.astype(jnp.float32), pre_gain).astype(jnp.bfloat16)
    gate_cast = gate_weight.astype(jnp.bfloat16)
    up_cast = up_weight.astype(jnp.bfloat16)
    gate_full, up_full = (
        lax.all_gather(gate_cast, "fs", axis=0, tiled=True),
        lax.all_gather(up_cast, "fs", axis=0, tiled=True),
    )
    piece = lax.all_gather(normed, "tp", axis=0, tiled=True)
    gate = jnp.dot(piece, gate_full, preferred_element_type=jnp.float32) * gate_scale
    up = jnp.dot(piece, up_full, preferred_element_type=jnp.float32) * up_scale
    hidden = (jax.nn.silu(gate) * up).astype(jnp.bfloat16)
    return (hidden, stream)


def solution(mesh):
    return jax.shard_map(
        on_device,
        mesh=mesh,
        in_specs=(
            P(("fs", "tp"), None),
            P(("fs", "tp"), None),
            P(),
            P(),
            P("fs", "tp"),
            P("fs", "tp"),
            P("tp"),
            P("tp"),
        ),
        out_specs=(P("fs", "tp"), P(("fs", "tp"), None)),
        check_vma=False,
    )
```

profile of v0, /device:TPU:0, one launch (start us, length us, event | category | flops | bytes accessed | tf_op | source)
XLA Modules:
  0.0 256.1 jit_solution(6884719773406794379)
XLA Ops:
  7.2 0.0 copy-start.1
  7.2 0.0 copy-start.3
  7.2 0.0 copy-start.2
  7.2 0.0 all-gather.6.cloned.1.call-start
  7.2 3.3 %convert_element_type.29 = bf16[1024,768]{1,0:T(8,128)(2,1)} convert(f32[1024,768]{1,0:T(8,128)} %param.12) | non-fusion elementwise | flops 786432 | bytes 4718592 | tf_op jit(solution)/shard_map/convert_element_type | solution.py:19
  10.6 0.0 copy-start.4
  10.6 0.0 all-gather.6.cloned.1.call-update
  10.6 0.0 all-gather.4.cloned.1.call-start
  10.6 0.0 copy-done.1
  10.6 0.3 fusion
  10.9 0.0 copy-done.3
  11.0 0.0 copy-done.2
  11.0 0.7 fusion.4
  11.7 0.0 copy-start
  11.7 0.0 copy-done.4
  11.7 1.3 fusion.6
  13.1 0.0 all-gather.4.cloned.1.call-update
  13.1 0.0 all-gather.8.cloned.1.call-start
  13.2 3.2 %convert_element_type.30 = bf16[1024,768]{1,0:T(8,128)(2,1)} convert(f32[1024,768]{1,0:T(8,128)} %param.13) | non-fusion elementwise | flops 786432 | bytes 4718592 | tf_op jit(solution)/shard_map/convert_element_type | solution.py:20
  16.4 0.0 copy-done
  16.4 0.0 all-gather.8.cloned.1.call-update
  16.4 0.0 copy-start.5
  16.4 0.0 copy-start.6
  16.4 67.1 %all-gather.6.cloned.1.call-done = bf16[4096,768]{1,0:T(8,128)(2,1)} async-done(((bf16[1024,768]{1,0:T(8,128)(2,1)}), bf16[4096,768]{1,0:T(8,128)(2,1)}) %all-gather.6.cloned.1.call-update) | async-done | bytes 6291472 | tf_op jit(solution)/shard_map/all_gather | solution.py:22
  83.5 83.7 %all-gather.4.cloned.1.call-done = bf16[1024,4096]{1,0:T(8,128)(2,1)} async-done(((bf16[128,4096]{1,0:T(8,128)(2,1)}), bf16[1024,4096]{1,0:T(8,128)(2,1)}) %all-gather.4.cloned.1.call-update) | async-done | bytes 8388624 | tf_op jit(solution)/shard_map/all_gather | solution.py:25
  167.2 10.9 %fusion.8 = f32[1024,768]{1,0:T(8,128)S(1)} fusion(bf16[1024,4096]{1,0:T(8,128)(2,1)} %all-gather.4.cloned.1.call-done, bf16[4096,768]{1,0:T(8,128)(2,1)} %all-gather.6.cloned.1.call-done), kind=kOutput, calls=%fused_computation.14 | convolution fusion | flops 6442450944 | bytes 17825792 | tf_op jit(solution)/shard_map/dot_general | solution.py:26
  178.1 59.5 %all-gather.8.cloned.1.call-done = bf16[4096,768]{1,0:T(8,128)(2,1)} async-done(((bf16[1024,768]{1,0:T(8,128)(2,1)}), bf16[4096,768]{1,0:T(8,128)(2,1)}) %all-gather.8.cloned.1.call-update) | async-done | bytes 6291472 | tf_op jit(solution)/shard_map/all_gather | solution.py:23
  237.6 0.0 copy-done.5
  237.6 0.0 copy-done.6
  237.6 12.1 %multiply_convert_fusion = bf16[1024,768]{1,0:T(8,128)(2,1)} fusion(f32[1024,768]{1,0:T(8,128)S(1)} %fusion.8, bf16[1024,4096]{1,0:T(8,128)(2,1)} %all-gather.4.cloned.1.call-done, bf16[4096,768]{1,0:T(8,128)(2,1)} %all-gather.8.cloned.1.call-done, f32[768]{0:T(1024)S(1)} %copy-done.5, f32[768]{0:T(1024)S(1)} %copy-done.6), kind=kOutput, calls=%fused_computation | convolution fusion | flops 6448742400 | bytes 19404800 | tf_op jit(solution)/shard_map/dot_general | solution.py:27
  (2 shorter events, 0.0 us)
Async XLA Ops:
  7.2 3.5 %copy-start.1 = (bf16[128,4096]{1,0:T(8,128)(2,1)S(1)}, bf16[128,4096]{1,0:T(8,128)(2,1)}, u32[]{:S(2)}) copy-start(bf16[128,4096]{1,0:T(8,128)(2,1)} %param.9) | copy-start | bytes 3145732
  7.2 3.8 %copy-start.3 = (f32[4096]{0:T(1024)S(1)}, f32[4096]{0:T(1024)}, u32[]{:S(2)}) copy-start(f32[4096]{0:T(1024)} %param.10) | copy-start | bytes 49156
  7.2 3.8 %copy-start.2 = (bf16[128,4096]{1,0:T(8,128)(2,1)S(1)}, bf16[128,4096]{1,0:T(8,128)(2,1)}, u32[]{:S(2)}) copy-start(bf16[128,4096]{1,0:T(8,128)(2,1)} %param.8) | copy-start | bytes 3145732
  7.2 76.3 %all-gather.6.cloned.1.call-start = ((), (), s32[]{:S(2)}) async-start(), calls=%async_computation.1 | async-start | bytes 7864320 | tf_op jit(solution)/shard_map/all_gather | solution.py:22
  10.6 1.2 copy-start.4
  10.6 156.6 %all-gather.4.cloned.1.call-start = ((), (), s32[]{:S(2)}) async-start(), calls=%async_computation | async-start | bytes 9437184 | tf_op jit(solution)/shard_map/all_gather | solution.py:25
  11.7 4.7 %copy-start = (bf16[128,4096]{1,0:T(8,128)(2,1)}, bf16[128,4096]{1,0:T(8,128)(2,1)S(1)}, u32[]{:S(2)}) copy-start(bf16[128,4096]{1,0:T(8,128)(2,1)S(1)} %get-tuple-element.3) | copy-start | bytes 3145732
  13.1 224.4 %all-gather.8.cloned.1.call-start = ((), (), s32[]{:S(2)}) async-start(), calls=%async_computation.2 | async-start | bytes 7864320 | tf_op jit(solution)/shard_map/all_gather | solution.py:23
  16.4 221.2 %copy-start.5 = (f32[768]{0:T(1024)S(1)}, f32[768]{0:T(1024)}, u32[]{:S(2)}) copy-start(f32[768]{0:T(1024)} %param.15) | copy-start | bytes 9220
  16.4 221.1 %copy-start.6 = (f32[768]{0:T(1024)S(1)}, f32[768]{0:T(1024)}, u32[]{:S(2)}) copy-start(f32[768]{0:T(1024)} %param.14) | copy-start | bytes 9220
Sparse Core Ops, SparseCore 0:
  10.7 72.7 all-gather.5
  85.1 82.0 all-gather.3
  169.0 68.5 all-gather.7
where the time goes:
time: 256 us
  waiting for transfers between devices  210 us (82%)
  matrix products  23 us (9%)
  between operations  13.8 us (5%)
  other arithmetic  8.92 us (3%)
    all_gather x1, waiting for transfers between devices, on_device(): piece = lax.all_gather(normed, 'tp', axis=0, tiled=True)  83.7 us
    all_gather x1, waiting for transfers between devices, on_device(): lax.all_gather(gate_cast, 'fs', axis=0, tiled=True)  67.1 us
    all_gather x1, waiting for transfers between devices, on_device(): lax.all_gather(up_cast, 'fs', axis=0, tiled=True)  59.5 us
    dot_general x1, matrix products, on_device(): up = jnp.dot(piece, up_full, preferred_element_type=jnp.float32) * up_scale  12.1 us
    dot_general x1, matrix products, on_device(): jnp.dot(piece, gate_full, preferred_element_type=jnp.float32) * gate_scale  10.9 us
  transfers between devices with their start and end apart: 3, of which 3 were waited for; matrix products, arithmetic and copies ran while one was open for 6% of the time, Pallas kernels for 0%

commit v1 on v0

--- a/solution.py
+++ b/solution.py
@@ -22,7 +22,12 @@
         lax.all_gather(gate_cast, "fs", axis=0, tiled=True),
         lax.all_gather(up_cast, "fs", axis=0, tiled=True),
     )
-    piece = lax.all_gather(normed, "tp", axis=0, tiled=True)
+    ring = [normed]
+    for hop in range(7):
+        ring.append(lax.ppermute(ring[-1], "tp", [(dev, (dev + 1) % 8) for dev in range(8)]))
+    piece = jnp.roll(
+        jnp.concatenate(ring[::-1], axis=0), (lax.axis_index("tp") + 1) * ring[0].shape[0], axis=0
+    )
     gate = jnp.dot(piece, gate_full, preferred_element_type=jnp.float32) * gate_scale
     up = jnp.dot(piece, up_full, preferred_element_type=jnp.float32) * up_scale
     hidden = (jax.nn.silu(gate) * up).astype(jnp.bfloat16)

time: 256 us -> 208 us (0.81)
  waiting for transfers between devices: 210 us -> 132 us
  local copies, waits for them, and re-layouts: 0.04 us -> 25.7 us
  other arithmetic: 8.92 us -> 11.6 us
    ppermute x0 -> x7, waiting for transfers between devices: none -> 112 us  [on_device(): lax.ppermute(ring[-1], 'tp', [(dev, (dev + 1) % 8) for dev in range(8)])]
    all_gather x1 -> x0, waiting for transfers between devices: 83.7 us -> none  [on_device(): piece = lax.all_gather(normed, 'tp', axis=0, tiled=True)]
    all_gather x1, waiting for transfers between devices: 67.1 us -> 0.01 us  [on_device(): lax.all_gather(gate_cast, 'fs', axis=0, tiled=True)]
    all_gather x1, waiting for transfers between devices: 59.5 us -> 20.6 us  [on_device(): lax.all_gather(up_cast, 'fs', axis=0, tiled=True)]
    unnamed x14 -> x36, local copies, waits for them, and re-layouts: 0.04 us -> 25.7 us
    reduce_sum x2, other arithmetic: 1.03 us -> 3.97 us  [rms_scaled(): jnp.mean(values * values, axis=-1, keepdims=True) + epsilon]
  transfers between devices with their start and end apart: 3 -> 9, of which waited for: 3 -> 8; matrix products, arithmetic and copies ran while one was open for 6% -> 20% of each run, Pallas kernels for 0% -> 0%
where the time goes in v1:
time: 208 us; the launch traced here: 207 us
  waiting for transfers between devices  132 us (63%)
  local copies, waits for them, and re-layouts  25.7 us (12%)
  matrix products  23 us (11%)
  between operations  14.1 us (7%)
  other arithmetic  11.6 us (6%)
    ppermute x7, waiting for transfers between devices, on_device(): lax.ppermute(ring[-1], 'tp', [(dev, (dev + 1) % 8) for dev in range(8)])  112 us
    unnamed x36, local copies, waits for them, and re-layouts  25.7 us
    all_gather x1, waiting for transfers between devices, on_device(): lax.all_gather(up_cast, 'fs', axis=0, tiled=True)  20.6 us
    dot_general x1, matrix products, on_device(): up = jnp.dot(piece, up_full, preferred_element_type=jnp.float32) * up_scale  12.1 us
    dot_general x1, matrix products, on_device(): jnp.dot(piece, gate_full, preferred_element_type=jnp.float32) * gate_scale  10.9 us
  transfers between devices with their start and end apart: 9, of which 8 were waited for; matrix products, arithmetic and copies ran while one was open for 20% of the time, Pallas kernels for 0%

profile of v1, /device:TPU:0, one launch (start us, length us, event | category | flops | bytes accessed | tf_op | source)
XLA Modules:
  0.0 207.3 jit_solution(7376714745754712901)
XLA Ops:
  7.2 0.0 copy-start.8
  7.2 0.0 all-gather.3.cloned.1.call-start
  7.2 3.2 %convert_element_type.29 = bf16[1024,768]{1,0:T(8,128)(2,1)} convert(f32[1024,768]{1,0:T(8,128)} %param.12) | non-fusion elementwise | flops 786432 | bytes 4718592 | tf_op jit(solution)/shard_map/convert_element_type | solution.py:19
  10.4 0.0 all-gather.3.cloned.1.call-update
  10.4 0.0 all-gather.5.cloned.1.call-start
  10.5 0.0 copy-start.7
  10.5 1.7 fusion.4
  12.2 2.3 %fusion.8 = (f32[128]{0:T(128)S(1)}, bf16[128,4096]{1,0:T(8,128)(2,1)S(1)}) fusion(f32[4096]{0:T(1024)} %param.10, f32[128]{0:T(128)S(1)} %add_rsqrt_fusion.1, bf16[128,4096]{1,0:T(8,128)(2,1)} %param.9, bf16[128,4096]{1,0:T(8,128)(2,1)} %param.8), kind=kLoop, calls=%fused_computation.13 | loop fusion | flops 4718464 | bytes 3163136 | tf_op jit(solution)/shard_map/reduce_sum | solution.py:10
  14.5 0.0 copy-start
  14.5 0.0 copy-done.8
  14.5 0.3 fusion.10
  14.9 0.5 collective-permute-start
  15.4 16.5 %collective-permute-done = bf16[128,4096]{1,0:T(8,128)(2,1)S(1)} collective-permute-done((bf16[128,4096]{1,0:T(8,128)(2,1)S(1)}, bf16[128,4096]{1,0:T(8,128)(2,1)S(1)}, u32[]{:S(2)}, u32[]{:S(2)}) %collective-permute-start) | collective-permute-done | bytes 1048608 | tf_op jit(solution)/shard_map/ppermute | solution.py:27
  31.9 0.0 collective-permute-start.1
  31.9 16.0 %collective-permute-done.1 = bf16[128,4096]{1,0:T(8,128)(2,1)S(1)} collective-permute-done((bf16[128,4096]{1,0:T(8,128)(2,1)S(1)}, bf16[128,4096]{1,0:T(8,128)(2,1)S(1)}, u32[]{:S(2)}, u32[]{:S(2)}) %collective-permute-start.1) | collective-permute-done | bytes 1048608 | tf_op jit(solution)/shard_map/ppermute | solution.py:27
  47.9 0.0 collective-permute-start.2
  47.9 16.0 %collective-permute-done.2 = bf16[128,4096]{1,0:T(8,128)(2,1)S(1)} collective-permute-done((bf16[128,4096]{1,0:T(8,128)(2,1)S(1)}, bf16[128,4096]{1,0:T(8,128)(2,1)S(1)}, u32[]{:S(2)}, u32[]{:S(2)}) %collective-permute-start.2) | collective-permute-done | bytes 1048608 | tf_op jit(solution)/shard_map/ppermute | solution.py:27
  64.0 0.0 copy-start.1
  64.0 1.0 copy-done.1
  64.9 0.0 collective-permute-start.3
  64.9 16.0 %collective-permute-done.3 = bf16[128,4096]{1,0:T(8,128)(2,1)S(1)} collective-permute-done((bf16[128,4096]{1,0:T(8,128)(2,1)S(1)}, bf16[128,4096]{1,0:T(8,128)(2,1)S(1)}, u32[]{:S(2)}, u32[]{:S(2)}) %collective-permute-start.3) | collective-permute-done | bytes 1048608 | tf_op jit(solution)/shard_map/ppermute | solution.py:27
  81.0 0.0 copy-start.3
  81.0 1.0 copy-done.3
  81.9 0.0 collective-permute-start.4
  81.9 16.0 %collective-permute-done.4 = bf16[128,4096]{1,0:T(8,128)(2,1)S(1)} collective-permute-done((bf16[128,4096]{1,0:T(8,128)(2,1)S(1)}, bf16[128,4096]{1,0:T(8,128)(2,1)S(1)}, u32[]{:S(2)}, u32[]{:S(2)}) %collective-permute-start.4) | collective-permute-done | bytes 1048608 | tf_op jit(solution)/shard_map/ppermute | solution.py:27
  97.9 0.0 copy-start.5
  97.9 1.0 copy-done.5
  98.9 0.0 collective-permute-start.5
  98.9 16.1 %collective-permute-done.5 = bf16[128,4096]{1,0:T(8,128)(2,1)} collective-permute-done((bf16[128,4096]{1,0:T(8,128)(2,1)S(1)}, bf16[128,4096]{1,0:T(8,128)(2,1)}, u32[]{:S(2)}, u32[]{:S(2)}) %collective-permute-start.5) | collective-permute-done | bytes 1048608 | tf_op jit(solution)/shard_map/ppermute | solution.py:27
  115.1 0.0 collective-permute-start.6
  115.1 0.0 copy-done.7
  115.1 1.4 convert_element_type.30
  116.4 0.0 all-gather.5.cloned.1.call-update
  116.5 0.0 copy-start.2
  116.5 14.9 %collective-permute-done.6 = bf16[128,4096]{1,0:T(8,128)(2,1)} collective-permute-done((bf16[128,4096]{1,0:T(8,128)(2,1)}, bf16[128,4096]{1,0:T(8,128)(2,1)}, u32[]{:S(2)}, u32[]{:S(2)}) %collective-permute-start.6) | collective-permute-done | bytes 1048608 | tf_op jit(solution)/shard_map/ppermute | solution.py:27
  131.4 2.3 %constant_dynamic-update-slice_fusion.15 = bf16[2048,4096]{1,0:T(8,128)(2,1)} fusion(bf16[128,4096]{1,0:T(8,128)(2,1)} %collective-permute-done.6), kind=kLoop, calls=%fused_computation.31 | loop fusion | bytes 2097152
  133.7 2.3 %constant_dynamic-update-slice_fusion.14 = bf16[2048,4096]{1,0:T(8,128)(2,1)} fusion(bf16[2048,4096]{1,0:T(8,128)(2,1)} %constant_dynamic-update-slice_fusion.15, bf16[128,4096]{1,0:T(8,128)(2,1)} %collective-permute-done.5), kind=kLoop, calls=%fused_computation.30 | loop fusion | bytes 2097152
  136.0 0.0 copy-start.6
  136.0 2.4 %constant_dynamic-update-slice_fusion.13 = bf16[2048,4096]{1,0:T(8,128)(2,1)} fusion(bf16[2048,4096]{1,0:T(8,128)(2,1)} %constant_dynamic-update-slice_fusion.14, bf16[128,4096]{1,0:T(8,128)(2,1)} %copy-done.5), kind=kLoop, calls=%fused_computation.29 | loop fusion | bytes 2097152
  138.4 0.0 copy-start.4
  138.4 2.4 %constant_dynamic-update-slice_fusion.12 = bf16[2048,4096]{1,0:T(8,128)(2,1)} fusion(bf16[2048,4096]{1,0:T(8,128)(2,1)} %constant_dynamic-update-slice_fusion.13, bf16[128,4096]{1,0:T(8,128)(2,1)} %copy-done.3), kind=kLoop, calls=%fused_computation.28 | loop fusion | bytes 2097152
  140.8 0.0 copy-done.2
  140.8 1.1 constant_dynamic-update-slice_fusion.11
  141.8 1.1 constant_dynamic-update-slice_fusion.10
  142.9 1.1 constant_dynamic-update-slice_fusion.9
  144.0 1.4 constant_dynamic-update-slice_fusion.8
  145.4 2.4 %constant_dynamic-update-slice_fusion.7 = bf16[2048,4096]{1,0:T(8,128)(2,1)} fusion(bf16[2048,4096]{1,0:T(8,128)(2,1)} %constant_dynamic-update-slice_fusion.8, bf16[128,4096]{1,0:T(8,128)(2,1)} %collective-permute-done.6), kind=kLoop, calls=%fused_computation.23 | loop fusion | bytes 2097152
  147.8 2.3 %constant_dynamic-update-slice_fusion.6 = bf16[2048,4096]{1,0:T(8,128)(2,1)} fusion(bf16[2048,4096]{1,0:T(8,128)(2,1)} %constant_dynamic-update-slice_fusion.7, bf16[128,4096]{1,0:T(8,128)(2,1)} %collective-permute-done.5), kind=kLoop, calls=%fused_computation.22 | loop fusion | bytes 2097152
  150.1 0.0 copy-done.6
  150.1 1.1 constant_dynamic-update-slice_fusion.5
  151.1 0.0 copy-done.4
  151.2 1.1 constant_dynamic-update-slice_fusion.4
  152.3 1.1 constant_dynamic-update-slice_fusion.3
  153.4 1.1 constant_dynamic-update-slice_fusion.2
  154.4 1.1 constant_dynamic-update-slice_fusion.1
  155.5 0.0 copy-done
  155.5 1.3 constant_dynamic-update-slice_fusion
  156.8 0.0 copy-start.9
  156.8 0.0 copy-start.10
  156.8 10.9 %fusion.2 = f32[1024,768]{1,0:T(8,128)S(1)} fusion(bf16[4096,768]{1,0:T(8,128)(2,1)} %all-gather.3.cloned.1.call-done, bf16[2048,4096]{1,0:T(8,128)(2,1)} %constant_dynamic-update-slice_fusion, s32[]{:T(128)S(6)} %select_n.14), kind=kOutput, calls=%fused_computation.2 | convolution fusion | flops 6442450944 | bytes 17825796 | tf_op jit(solution)/shard_map/dot_general | solution.py:31
  167.8 20.6 %all-gather.5.cloned.1.call-done = bf16[4096,768]{1,0:T(8,128)(2,1)} async-done(((bf16[1024,768]{1,0:T(8,128)(2,1)}), bf16[4096,768]{1,0:T(8,128)(2,1)}) %all-gather.5.cloned.1.call-update) | async-done | bytes 6291472 | tf_op jit(solution)/shard_map/all_gather | solution.py:23
  188.3 0.0 copy-done.9
  188.3 0.0 copy-done.10
  188.3 12.1 %multiply_convert_fusion = bf16[1024,768]{1,0:T(8,128)(2,1)} fusion(f32[1024,768]{1,0:T(8,128)S(1)} %fusion.2, bf16[4096,768]{1,0:T(8,128)(2,1)} %all-gather.5.cloned.1.call-done, bf16[2048,4096]{1,0:T(8,128)(2,1)} %constant_dynamic-update-slice_fusion, s32[]{:T(128)S(6)} %select_n.14, f32[768]{0:T(1024)S(1)} %copy-done.9, f32[768]{0:T(1024)S(1)} %copy-done.10), kind=kOutput, calls=%fused_computation.4 | convolution fusion | flops 6448742400 | bytes 19404804 | tf_op jit(solution)/shard_map/dot_general | solution.py:32
  (3 shorter events, 0.0 us)
Async XLA Ops:
  7.2 7.3 %copy-start.8 = (f32[4096]{0:T(1024)S(1)}, f32[4096]{0:T(1024)}, u32[]{:S(2)}) copy-start(f32[4096]{0:T(1024)} %param.11) | copy-start | bytes 49156
  7.2 149.7 %all-gather.3.cloned.1.call-start = ((), (), s32[]{:S(2)}) async-start(), calls=%async_computation | async-start | bytes 7864320 | tf_op jit(solution)/shard_map/all_gather | solution.py:22
  10.4 177.9 %all-gather.5.cloned.1.call-start = ((), (), s32[]{:S(2)}) async-start(), calls=%async_computation.1 | async-start | bytes 7864320 | tf_op jit(solution)/shard_map/all_gather | solution.py:23
  10.5 104.6 %copy-start.7 = (f32[1024,768]{1,0:T(8,128)S(1)}, f32[1024,768]{1,0:T(8,128)}, u32[]{:S(2)}) copy-start(f32[1024,768]{1,0:T(8,128)} %param.13) | copy-start | bytes 9437188
  14.5 141.0 %copy-start = (bf16[128,4096]{1,0:T(8,128)(2,1)}, bf16[128,4096]{1,0:T(8,128)(2,1)S(1)}, u32[]{:S(2)}) copy-start(bf16[128,4096]{1,0:T(8,128)(2,1)S(1)} %get-tuple-element.3) | copy-start | bytes 3145732
  14.9 17.1 %collective-permute-start = (bf16[128,4096]{1,0:T(8,128)(2,1)S(1)}, bf16[128,4096]{1,0:T(8,128)(2,1)S(1)}, u32[]{:S(2)}, u32[]{:S(2)}) collective-permute-start(bf16[128,4096]{1,0:T(8,128)(2,1)S(1)} %fusion.10), channel_id=1, source_target_pairs={{0,1},{1,2},{2,3},{3,4},{4,5},{5,6},{6,7},{7,0},{8,9},{9,10},{10,1... | collective-permute-start | bytes 3145736 | tf_op jit(solution)/shard_map/ppermute | solution.py:27
  31.9 16.0 %collective-permute-start.1 = (bf16[128,4096]{1,0:T(8,128)(2,1)S(1)}, bf16[128,4096]{1,0:T(8,128)(2,1)S(1)}, u32[]{:S(2)}, u32[]{:S(2)}) collective-permute-start(bf16[128,4096]{1,0:T(8,128)(2,1)S(1)} %collective-permute-done), channel_id=1, source_target_pairs={{0,1},{1,2},{2,3},{3,4},{4,5},{5,6},{6,7},{7,0},{8,9},{9,10},{10,1... | collective-permute-start | bytes 3145736 | tf_op jit(solution)/shard_map/ppermute | solution.py:27
  47.9 16.0 %collective-permute-start.2 = (bf16[128,4096]{1,0:T(8,128)(2,1)S(1)}, bf16[128,4096]{1,0:T(8,128)(2,1)S(1)}, u32[]{:S(2)}, u32[]{:S(2)}) collective-permute-start(bf16[128,4096]{1,0:T(8,128)(2,1)S(1)} %collective-permute-done.1), channel_id=1, source_target_pairs={{0,1},{1,2},{2,3},{3,4},{4,5},{5,6},{6,7},{7,0},{8,9},{9,10},{10,1... | collective-permute-start | bytes 3145736 | tf_op jit(solution)/shard_map/ppermute | solution.py:27
  64.0 1.0 copy-start.1
  64.9 16.0 %collective-permute-start.3 = (bf16[128,4096]{1,0:T(8,128)(2,1)S(1)}, bf16[128,4096]{1,0:T(8,128)(2,1)S(1)}, u32[]{:S(2)}, u32[]{:S(2)}) collective-permute-start(bf16[128,4096]{1,0:T(8,128)(2,1)S(1)} %collective-permute-done.2), channel_id=1, source_target_pairs={{0,1},{1,2},{2,3},{3,4},{4,5},{5,6},{6,7},{7,0},{8,9},{9,10},{10,1... | collective-permute-start | bytes 3145736 | tf_op jit(solution)/shard_map/ppermute | solution.py:27
  81.0 1.0 copy-start.3
  81.9 16.0 %collective-permute-start.4 = (bf16[128,4096]{1,0:T(8,128)(2,1)S(1)}, bf16[128,4096]{1,0:T(8,128)(2,1)S(1)}, u32[]{:S(2)}, u32[]{:S(2)}) collective-permute-start(bf16[128,4096]{1,0:T(8,128)(2,1)S(1)} %collective-permute-done.3), channel_id=1, source_target_pairs={{0,1},{1,2},{2,3},{3,4},{4,5},{5,6},{6,7},{7,0},{8,9},{9,10},{10,1... | collective-permute-start | bytes 3145736 | tf_op jit(solution)/shard_map/ppermute | solution.py:27
  97.9 1.0 copy-start.5
  98.9 16.1 %collective-permute-start.5 = (bf16[128,4096]{1,0:T(8,128)(2,1)S(1)}, bf16[128,4096]{1,0:T(8,128)(2,1)}, u32[]{:S(2)}, u32[]{:S(2)}) collective-permute-start(bf16[128,4096]{1,0:T(8,128)(2,1)S(1)} %collective-permute-done.4), channel_id=1, source_target_pairs={{0,1},{1,2},{2,3},{3,4},{4,5},{5,6},{6,7},{7,0},{8,9},{9,10},{10,1... | collective-permute-start | bytes 3145736 | tf_op jit(solution)/shard_map/ppermute | solution.py:27
  115.1 16.3 %collective-permute-start.6 = (bf16[128,4096]{1,0:T(8,128)(2,1)}, bf16[128,4096]{1,0:T(8,128)(2,1)}, u32[]{:S(2)}, u32[]{:S(2)}) collective-permute-start(bf16[128,4096]{1,0:T(8,128)(2,1)} %collective-permute-done.5), channel_id=1, source_target_pairs={{0,1},{1,2},{2,3},{3,4},{4,5},{5,6},{6,7},{7,0},{8,9},{9,10},{10,1... | collective-permute-start | bytes 3145736 | tf_op jit(solution)/shard_map/ppermute | solution.py:27
  116.5 24.3 %copy-start.2 = (bf16[128,4096]{1,0:T(8,128)(2,1)S(1)}, bf16[128,4096]{1,0:T(8,128)(2,1)}, u32[]{:S(2)}) copy-start(bf16[128,4096]{1,0:T(8,128)(2,1)} %copy-done.1) | copy-start | bytes 3145732
  136.0 14.1 %copy-start.6 = (bf16[128,4096]{1,0:T(8,128)(2,1)S(1)}, bf16[128,4096]{1,0:T(8,128)(2,1)}, u32[]{:S(2)}) copy-start(bf16[128,4096]{1,0:T(8,128)(2,1)} %copy-done.5) | copy-start | bytes 3145732
  138.4 12.8 %copy-start.4 = (bf16[128,4096]{1,0:T(8,128)(2,1)S(1)}, bf16[128,4096]{1,0:T(8,128)(2,1)}, u32[]{:S(2)}) copy-start(bf16[128,4096]{1,0:T(8,128)(2,1)} %copy-done.3) | copy-start | bytes 3145732
  156.8 31.5 %copy-start.9 = (f32[768]{0:T(1024)S(1)}, f32[768]{0:T(1024)}, u32[]{:S(2)}) copy-start(f32[768]{0:T(1024)} %param.15) | copy-start | bytes 9220
  156.8 31.5 %copy-start.10 = (f32[768]{0:T(1024)S(1)}, f32[768]{0:T(1024)}, u32[]{:S(2)}) copy-start(f32[768]{0:T(1024)} %param.14) | copy-start | bytes 9220
Sparse Core Ops, SparseCore 0:
  10.6 72.7 all-gather.2
  116.6 71.7 all-gather.4
